TPU v7x, 32 devices: a whole 2x2x4 slice. The times are simulated.
32 devices in a mesh: sp: 8 (over z, y), tp: 4 (over x, core).
Axes of the slice: x: 2, y: 2, z: 4, core: 2. Of those that a mesh axis runs over, the one named last changes fastest.
Arguments:
- residual: bfloat16 [4096, 2048], P(('sp', 'tp')), may hold values from -6 to 6
- query_major: bfloat16 [4096, 1024], P('sp', 'tp'), may hold values from -160 to 160
- keys_major: bfloat16 [4096, 1024], P('sp', 'tp'), may hold values from -6.5 to 6.5
- values_major: bfloat16 [4096, 1024], P('sp', 'tp'), may hold values from -6 to 6
- query_minor: bfloat16 [4096, 512], P('sp', 'tp'), may hold values from -160 to 160
- keys_minor: bfloat16 [4096, 512], P('sp', 'tp'), may hold values from -6.5 to 6.5
- values_minor: bfloat16 [4096, 512], P('sp', 'tp'), may hold values from -6 to 6
- lambda_major: float32 [8], P('tp'), may hold values from 0.3 to 0.8
- lambda_minor: float32 [8], P('tp'), may hold values from 0.3 to 0.8
- gain_major: float32 [128], replicated, may hold values from 0.1 to 1.9
- gain_minor: float32 [64], replicated, may hold values from 0.1 to 1.9
- output_major: bfloat16 [1024, 2048], P('tp'), may hold values from -0.15625 to 0.15625
- output_minor: bfloat16 [512, 2048], P('tp'), may hold values from -0.15625 to 0.15625
- mixer_gain: float32 [2048], replicated, may hold values from 0.1 to 1.9
- up_weight: bfloat16 [2048, 8192], P('sp', 'tp'), may hold values from -0.125 to 0.125
- down_weight: bfloat16 [8192, 2048], P('tp', 'sp'), may hold values from -0.0625 to 0.0625
Outputs:
- layer_out: bfloat16 [4096, 2048], P(('sp', 'tp'))
All inputs are finite; a program needn't handle non-finite values.
Results may differ from a plain program's by a relative error of at most 0.018.
Values may be sent and summed in bfloat16 or wider, within the bound.
A program may use at most 128 MiB of HBM per device.

v0:
```python
import jax
import jax.numpy as jnp
from jax import lax
from jax.sharding import PartitionSpec as P

DK_MAJOR = 64
DK_MINOR = 32
SEGMENT = 64
EPSILON = 1e-06
NEGATIVE = -1e30


def swapped(value, axis, stride):
    mask = 2**stride
    pairs = [(source, source ^ mask) for source in range(lax.axis_size(axis))]
    return lax.ppermute(value, axis, pairs)


def to_wire(value):
    return lax.optimization_barrier(value.astype(jnp.bfloat16)).astype(jnp.float32)


def fresh(head_count, query_count, value_size):
    return (
        jnp.full((head_count, 2, query_count), NEGATIVE, jnp.float32),
        jnp.zeros((head_count, 2, query_count), jnp.float32),
        jnp.zeros((head_count, 2, query_count, value_size), jnp.float32),
    )


def fold_piece(carried, queries, key_rows, values, query_pos, key_size):
    head_count = key_rows.shape[1] // (2 * key_size)
    value_size = values.shape[1] // head_count
    query_count = queries.shape[0]
    block_len = min(key_rows.shape[0], query_count)
    query_heads = queries.reshape(query_count, head_count, 2, key_size)
    last_segment = query_pos[query_count - 1] // SEGMENT

    def visit(block_id, carried_in):
        key_first = block_id * block_len

        def update(running):
            peak_old, total_old, accum_old = running
            keys_block = lax.dynamic_slice_in_dim(key_rows, key_first, block_len, 0)
            keys_block = keys_block.reshape(block_len, head_count, 2, key_size)
            values_block = lax.dynamic_slice_in_dim(values, key_first, block_len, 0)
            values_block = values_block.reshape(block_len, head_count, value_size)
            key_pos = key_first + jnp.arange(block_len, dtype=jnp.int32)
            visible = key_pos[None, :] // SEGMENT <= query_pos[:, None] // SEGMENT
            scores = jnp.einsum(
                "qhmd,khmd->hmqk", query_heads, keys_block, preferred_element_type=jnp.float32
            ) * key_size ** (-0.5)
            scores = jnp.where(visible, scores, NEGATIVE)
            peak_new = jnp.maximum(peak_old, jnp.max(scores, axis=-1))
            weights = jnp.where(visible, jnp.exp(scores - peak_new[..., None]), 0.0)
            factor = jnp.exp(peak_old - peak_new)
            total_new = total_old * factor + jnp.sum(weights, axis=-1)
            accum_new = accum_old * factor[..., None] + jnp.einsum(
                "hmqk,khe->hmqe",
                weights.astype(jnp.bfloat16),
                values_block,
                preferred_element_type=jnp.float32,
            )
            return (peak_new, total_new, accum_new)

        def unchanged(running):
            return running

        block_segment = key_first // SEGMENT
        return lax.cond(block_segment <= last_segment, update, unchanged, carried_in)

    return lax.fori_loop(0, key_rows.shape[0] // block_len, visit, carried)


def finish(carried, lambdas, scaling):
    peak_unused, totals, accum = carried
    output = (
        accum[:, 0] / totals[:, 0, :, None]
        - lambdas[:, None, None] * accum[:, 1] / totals[:, 1, :, None]
    )
    output = (
        output * lax.rsqrt(jnp.mean(output * output, axis=-1, keepdims=True) + EPSILON) * scaling
    )
    head_count, query_count, value_size = output.shape
    return (
        jnp.transpose(output, (1, 0, 2))
        .reshape(query_count, head_count * value_size)
        .astype(jnp.bfloat16)
    )


def normalize(stream, scaling):
    normed = (
        stream * lax.rsqrt(jnp.mean(stream * stream, axis=-1, keepdims=True) + EPSILON) * scaling
    )
    return normed.astype(jnp.bfloat16)


def body(
    residual,
    query_major,
    keys_major,
    values_major,
    query_minor,
    keys_minor,
    values_minor,
    lambda_major,
    lambda_minor,
    gain_major,
    gain_minor,
    output_major,
    output_minor,
    mixer_gain,
    up_weight,
    down_weight,
):
    query_count = query_major.shape[0]
    half_rows = query_count // 2
    own_index = lax.axis_index("sp")
    sp_count = lax.axis_size("sp")
    sp_bits = sp_count.bit_length() - 1
    width_major = query_major.shape[1]
    early_pos = own_index * query_count + jnp.arange(half_rows, dtype=jnp.int32)
    early_major = query_major[:half_rows]
    early_minor = query_minor[:half_rows]
    late_queries = jnp.concatenate([query_major[half_rows:], query_minor[half_rows:]], axis=1)
    for bit_number in range(sp_bits):
        late_queries = swapped(late_queries, "sp", bit_number)
    late_major = late_queries[:, :width_major]
    late_minor = late_queries[:, width_major:]
    late_pos = (
        (sp_count - 1 - own_index) * query_count
        + half_rows
        + jnp.arange(half_rows, dtype=jnp.int32)
    )
    heads_major = keys_major.shape[1] // (2 * DK_MAJOR)
    heads_minor = keys_minor.shape[1] // (2 * DK_MINOR)
    size_major = values_major.shape[1] // heads_major
    size_minor = values_minor.shape[1] // heads_minor
    init_major = (
        fresh(heads_major, half_rows, size_major),
        fresh(heads_major, half_rows, size_major),
    )
    init_minor = (
        fresh(heads_minor, half_rows, size_minor),
        fresh(heads_minor, half_rows, size_minor),
    )
    pieces = (
        lax.all_gather(keys_major, "sp", axis=0, tiled=True),
        lax.all_gather(values_major, "sp", axis=0, tiled=True),
    )
    fold_pieces = (
        lax.all_gather(keys_minor, "sp", axis=0, tiled=True),
        lax.all_gather(values_minor, "sp", axis=0, tiled=True),
    )
    first_major = finish(
        fold_piece(init_major[0], early_major, pieces[0], pieces[1], early_pos, DK_MAJOR),
        lambda_major,
        gain_major,
    )
    first_minor = finish(
        fold_piece(init_minor[0], early_minor, fold_pieces[0], fold_pieces[1], early_pos, DK_MINOR),
        lambda_minor,
        gain_minor,
    )
    second_major = finish(
        fold_piece(init_major[1], late_major, pieces[0], pieces[1], late_pos, DK_MAJOR),
        lambda_major,
        gain_major,
    )
    second_minor = finish(
        fold_piece(init_minor[1], late_minor, fold_pieces[0], fold_pieces[1], late_pos, DK_MINOR),
        lambda_minor,
        gain_minor,
    )
    out_width = second_major.shape[1]
    late_out = jnp.concatenate([second_major, second_minor], axis=1)
    for bit_number in range(sp_bits):
        late_out = swapped(late_out, "sp", bit_number)
    second_major = late_out[:, :out_width]
    second_minor = late_out[:, out_width:]
    out_major = jnp.concatenate([first_major, second_major], axis=0)
    out_minor = jnp.concatenate([first_minor, second_minor], axis=0)
    partial_sum = jnp.dot(out_major, output_major, preferred_element_type=jnp.float32)
    partial_sum = partial_sum + jnp.dot(out_minor, output_minor, preferred_element_type=jnp.float32)
    mixed = lax.psum_scatter(
        to_wire(partial_sum).astype(jnp.bfloat16), "tp", scatter_dimension=0, tiled=True
    ).astype(jnp.float32)
    stream = residual.astype(jnp.float32) + mixed
    normed_all = lax.all_gather(normalize(stream, mixer_gain), "tp", axis=0, tiled=True)
    pre_act = jnp.dot(
        normed_all,
        lax.all_gather(up_weight, "sp", axis=0, tiled=True),
        preferred_element_type=jnp.float32,
    )
    hidden = jnp.square(jax.nn.relu(pre_act)).astype(jnp.bfloat16)
    down_full = lax.all_gather(down_weight, "sp", axis=1, tiled=True)
    down_sum = lax.psum_scatter(
        to_wire(jnp.dot(hidden, down_full, preferred_element_type=jnp.float32)).astype(
            jnp.bfloat16
        ),
        "tp",
        scatter_dimension=0,
        tiled=True,
    ).astype(jnp.float32)
    return (stream + down_sum).astype(jnp.bfloat16)


def solution(mesh):
    return jax.shard_map(
        body,
        mesh=mesh,
        in_specs=(
            P(("sp", "tp"), None),
            P("sp", "tp"),
            P("sp", "tp"),
            P("sp", "tp"),
            P("sp", "tp"),
            P("sp", "tp"),
            P("sp", "tp"),
            P("tp"),
            P("tp"),
            P(),
            P(),
            P("tp", None),
            P("tp", None),
            P(),
            P("sp", "tp"),
            P("tp", "sp"),
        ),
        out_specs=P(("sp", "tp"), None),
        check_vma=False,
    )
```

profile of v0, /device:TPU:0, one launch (start us, length us, event | category | flops | bytes accessed | tf_op | source)
XLA Modules:
  0.0 631.5 jit_solution(7971657574266542645)
XLA Ops:
  15.8 3.1 collective-permute-start
  18.8 6.3 collective-permute-done
  26.9 4.9 collective-permute-done.1
  31.9 3.2 collective-permute-start.2
  41.7 3.5 collective-permute-done.2
  45.5 9.6 %all-gather.12.cloned.1.call-done = bf16[4096,128]{0,1:T(8,128)(2,1)} async-done(((bf16[512,128]{0,1:T(8,128)(2,1)}), bf16[4096,128]{0,1:T(8,128)(2,1)}) %all-gather.12.cloned.1.call-update) | async-done | bytes 1048592 | tf_op jit(solution)/shard_map/all_gather | solution.py:153
  55.0 42.4 %all-gather.14.cloned.1.call-done = bf16[4096,128]{0,1:T(8,128)(2,1)} async-done(((bf16[512,128]{0,1:T(8,128)(2,1)}), bf16[4096,128]{0,1:T(8,128)(2,1)}) %all-gather.14.cloned.1.call-update) | async-done | bytes 1048592 | tf_op jit(solution)/shard_map/all_gather | solution.py:154
  97.5 33.4 %while.82 = (s32[]{:T(128)}, f32[2,2,256]{2,1,0:T(2,128)S(1)}, f32[2,2,256]{2,1,0:T(2,128)S(1)}, f32[2,2,256,64]{2,3,1,0:T(8,128)S(1)}, s32[]{:T(128)}, /*index=...) while((s32[]{:T(128)}, f32[2,2,256]{2,1,0:T(2,128)S(1)}, ...), condition=%wide.region_19.20_spmd.clone, body=%wide.region_14.19_spmd.clone.sunk | while | flops 52897816 | bytes 4463083 | solution.py:72
  99.6 2.0 conditional.14
  101.7 2.0 conditional.14
  105.9 2.0 conditional.14
  108.0 2.0 conditional.14
  112.2 2.0 conditional.14
  126.8 2.0 conditional.14
  131.0 3.3 while.83
  134.6 14.2 %all-gather.10.cloned.1.call-done = bf16[4096,256]{0,1:T(8,128)(2,1)} async-done(((bf16[512,256]{0,1:T(8,128)(2,1)}), bf16[4096,256]{0,1:T(8,128)(2,1)}) %all-gather.10.cloned.1.call-update) | async-done | bytes 2097168 | tf_op jit(solution)/shard_map/all_gather | solution.py:150
  148.8 50.5 %all-gather.8.cloned.1.call-done = bf16[4096,256]{0,1:T(8,128)(2,1)} async-done(((bf16[512,256]{0,1:T(8,128)(2,1)}), bf16[4096,256]{0,1:T(8,128)(2,1)}) %all-gather.8.cloned.1.call-update) | async-done | bytes 2097168 | tf_op jit(solution)/shard_map/all_gather | solution.py:149
  199.4 38.5 %while.81 = (s32[]{:T(128)}, f32[2,2,256]{2,1,0:T(2,128)S(1)}, f32[2,2,256]{2,1,0:T(2,128)S(1)}, f32[2,2,256,128]{3,2,1,0:T(8,128)S(1)}, s32[]{:T(128)}, /*index...) while((s32[]{:T(128)}, f32[2,2,256]{2,1,0:T(2,128)S(1)}, ...), condition=%wide.region_12.13_spmd.clone, body=%wide.region_7.12_spmd.clone.sunk | while | flops 103360528 | bytes 5446123 | solution.py:72
  199.4 2.3 conditional.13
  201.8 2.3 conditional.13
  204.2 2.3 conditional.13
  206.6 2.3 conditional.13
  209.1 2.3 conditional.13
  211.5 2.3 conditional.13
  213.9 2.3 conditional.13
  216.3 2.3 conditional.13
  218.7 2.3 conditional.13
  221.1 2.3 conditional.13
  223.5 2.3 conditional.13
  225.9 2.3 conditional.13
  228.3 2.3 conditional.13
  230.7 2.3 conditional.13
  233.1 2.3 conditional.13
  235.5 2.3 conditional.13
  238.0 3.6 while.80
  238.0 2.4 conditional.12
  245.2 5.0 collective-permute-done.3
  250.2 5.7 collective-permute-done.4
  256.9 8.6 %collective-permute-done.5 = bf16[256,384]{0,1:T(8,128)(2,1)S(1)} collective-permute-done((bf16[256,384]{0,1:T(8,128)(2,1)S(1)}, bf16[256,384]{0,1:T(8,128)(2,1)S(1)}, u32[]{:S(2)}, u32[]{:S(2)}) %collective-permute-start.5) | collective-permute-done | bytes 196640 | tf_op jit(solution)/shard_map/ppermute | solution.py:16
  266.2 2.1 add_convert_fusion
  268.4 30.5 %reduce-scatter.3.cloned.1.call-done = bf16[128,2048]{1,0:T(8,128)(2,1)} async-done(((bf16[512,2048]{1,0:T(8,128)(2,1)}), bf16[128,2048]{1,0:T(8,128)(2,1)}) %reduce-scatter.3.cloned.1.call-update) | async-done | bytes 524304 | tf_op jit(solution)/shard_map/reduce_scatter | solution.py:186
  300.2 2.0 multiply_convert_fusion.1
  304.0 21.0 %all-gather.16.cloned.1.call-done = bf16[512,2048]{1,0:T(8,128)(2,1)} async-done(((bf16[128,2048]{1,0:T(8,128)(2,1)}), bf16[512,2048]{1,0:T(8,128)(2,1)}) %all-gather.16.cloned.1.call-update) | async-done | bytes 2097168 | tf_op jit(solution)/shard_map/all_gather | solution.py:190
  325.0 126.6 %all-gather.18.cloned.1.call-done = bf16[2048,2048]{1,0:T(8,128)(2,1)} async-done(((bf16[256,2048]{1,0:T(8,128)(2,1)}), bf16[2048,2048]{1,0:T(8,128)(2,1)}) %all-gather.18.cloned.1.call-update) | async-done | bytes 8388624 | tf_op jit(solution)/shard_map/all_gather | solution.py:193
  451.6 125.2 %all-gather.20.cloned.1.call-done = bf16[2048,2048]{1,0:T(8,128)(2,1)} async-done(((bf16[2048,256]{1,0:T(8,128)(2,1)}), bf16[2048,2048]{1,0:T(8,128)(2,1)}) %all-gather.20.cloned.1.call-update) | async-done | bytes 8388624 | tf_op jit(solution)/shard_map/all_gather | solution.py:197
  576.8 16.5 %convolution_convert_fusion = bf16[512,2048]{1,0:T(8,128)(2,1)} fusion(bf16[2048,2048]{1,0:T(8,128)(2,1)} %all-gather.20.cloned.1.call-done, bf16[512,2048]{1,0:T(8,128)(2,1)} %all-gather.16.cloned.1.call-done, bf16[2048,2048]{1,0:T(8,128)(2,1)} %all-gather.18.cloned.1.call-done), kind=kOutput, calls=%fused_computation.102 | convolution fusion | flops 8594128896 | bytes 20971520 | tf_op jit(solution)/shard_map/dot_general | solution.py:199
  593.4 29.5 %reduce-scatter.5.cloned.1.call-done = bf16[128,2048]{1,0:T(8,128)(2,1)} async-done(((bf16[512,2048]{1,0:T(8,128)(2,1)}), bf16[128,2048]{1,0:T(8,128)(2,1)}) %reduce-scatter.5.cloned.1.call-update) | async-done | bytes 524304 | tf_op jit(solution)/shard_map/reduce_scatter | solution.py:198
  622.9 2.1 add_convert_fusion.1
  (500 shorter events, 116.3 us)
Async XLA Ops:
  6.5 259.7 %copy-start = (bf16[256,2048]{1,0:T(8,128)(2,1)S(1)}, bf16[256,2048]{1,0:T(8,128)(2,1)}, u32[]{:S(2)}) copy-start(bf16[256,2048]{1,0:T(8,128)(2,1)} %param.43) | copy-start | bytes 3145732
  6.5 48.5 %all-gather.12.cloned.1.call-start = ((), (), s32[]{:S(2)}) async-start(), calls=%async_computation.4 | async-start | bytes 1179648 | tf_op jit(solution)/shard_map/all_gather | solution.py:153
  8.3 89.1 %all-gather.14.cloned.1.call-start = ((), (), s32[]{:S(2)}) async-start(), calls=%async_computation.5 | async-start | bytes 1179648 | tf_op jit(solution)/shard_map/all_gather | solution.py:154
  10.1 138.8 %all-gather.10.cloned.1.call-start = ((), (), s32[]{:S(2)}) async-start(), calls=%async_computation.3 | async-start | bytes 2359296 | tf_op jit(solution)/shard_map/all_gather | solution.py:150
  11.9 187.4 %all-gather.8.cloned.1.call-start = ((), (), s32[]{:S(2)}) async-start(), calls=%async_computation.2 | async-start | bytes 2359296 | tf_op jit(solution)/shard_map/all_gather | solution.py:149
  13.8 285.1 %reduce-scatter.3.cloned.1.call-start = ((), (), s32[]{:S(2)}) async-start(), calls=%async_computation.6 | async-start | bytes 2621440 | tf_op jit(solution)/shard_map/reduce_scatter | solution.py:186
  15.8 9.4 %collective-permute-start = (bf16[256,384]{1,0:T(8,128)(2,1)S(1)}, bf16[256,384]{1,0:T(8,128)(2,1)S(1)}, u32[]{:S(2)}, u32[]{:S(2)}) collective-permute-start(bf16[256,384]{1,0:T(8,128)(2,1)S(1)} %pad_maximum_fusion), channel_id=1, source_target_pairs={{0,4},{4,0},{8,12},{12,8},{16,20},{20,16},{24,28},{28,24},{1,5},{5... | collective-permute-start | bytes 589832 | tf_op jit(solution)/shard_map/ppermute | solution.py:16
  25.1 6.7 %collective-permute-start.1 = (bf16[256,384]{1,0:T(8,128)(2,1)S(1)}, bf16[256,384]{1,0:T(8,128)(2,1)S(1)}, u32[]{:S(2)}, u32[]{:S(2)}) collective-permute-start(bf16[256,384]{1,0:T(8,128)(2,1)S(1)} %collective-permute-done), channel_id=1, source_target_pairs={{0,8},{4,12},{8,0},{12,4},{16,24},{20,28},{24,16},{28,20},{1,9},{5... | collective-permute-start | bytes 589832 | tf_op jit(solution)/shard_map/ppermute | solution.py:16
  31.9 13.4 %collective-permute-start.2 = (bf16[256,384]{1,0:T(8,128)(2,1)S(1)}, bf16[256,384]{1,0:T(8,128)(2,1)S(1)}, u32[]{:S(2)}, u32[]{:S(2)}) collective-permute-start(bf16[256,384]{1,0:T(8,128)(2,1)S(1)} %collective-permute-done.1), channel_id=1, source_target_pairs={{0,16},{4,20},{8,24},{12,28},{16,0},{20,4},{24,8},{28,12},{1,17},{... | collective-permute-start | bytes 589832 | tf_op jit(solution)/shard_map/ppermute | solution.py:16
  131.0 3.4 copy-start.6
  131.0 3.5 copy-start.5
  241.6 23.9 %copy-start.3 = (bf16[128,2048]{1,0:T(8,128)(2,1)S(1)}, bf16[128,2048]{1,0:T(8,128)(2,1)}, u32[]{:S(2)}) copy-start(bf16[128,2048]{1,0:T(8,128)(2,1)} %param.44) | copy-start | bytes 1572868
  243.7 6.5 %collective-permute-start.3 = (bf16[256,384]{0,1:T(8,128)(2,1)S(1)}, bf16[256,384]{0,1:T(8,128)(2,1)S(1)}, u32[]{:S(2)}, u32[]{:S(2)}) collective-permute-start(bf16[256,384]{0,1:T(8,128)(2,1)S(1)} %pad_maximum_fusion.1), channel_id=1, source_target_pairs={{0,4},{4,0},{8,12},{12,8},{16,20},{20,16},{24,28},{28,24},{1,5},{5... | collective-permute-start | bytes 589832 | tf_op jit(solution)/shard_map/ppermute | solution.py:16
  250.2 5.7 collective-permute-start.4
  255.9 9.6 %collective-permute-start.5 = (bf16[256,384]{0,1:T(8,128)(2,1)S(1)}, bf16[256,384]{0,1:T(8,128)(2,1)S(1)}, u32[]{:S(2)}, u32[]{:S(2)}) collective-permute-start(bf16[256,384]{0,1:T(8,128)(2,1)S(1)} %collective-permute-done.4), channel_id=1, source_target_pairs={{0,16},{4,20},{8,24},{12,28},{16,0},{20,4},{24,8},{28,12},{1,17},{... | collective-permute-start | bytes 589832 | tf_op jit(solution)/shard_map/ppermute | solution.py:16
  266.2 32.7 %copy-start.1 = (bf16[128,2048]{1,0:T(8,128)(2,1)S(1)}, bf16[128,2048]{1,0:T(8,128)(2,1)}, u32[]{:S(2)}) copy-start(bf16[128,2048]{1,0:T(8,128)(2,1)} %param.32) | copy-start | bytes 1572868
  266.2 34.0 %copy-start.4 = (f32[2048]{0:T(1024)S(1)}, f32[2048]{0:T(1024)}, u32[]{:S(2)}) copy-start(f32[2048]{0:T(1024)} %param.45) | copy-start | bytes 24580
  268.4 56.6 %all-gather.16.cloned.1.call-start = ((), (), s32[]{:S(2)}) async-start(), calls=%async_computation.7 | async-start | bytes 2621440 | tf_op jit(solution)/shard_map/all_gather | solution.py:190
  302.3 149.4 %all-gather.18.cloned.1.call-start = ((), (), s32[]{:S(2)}) async-start(), calls=%async_computation.8 | async-start | bytes 9437184 | tf_op jit(solution)/shard_map/all_gather | solution.py:193
  303.0 273.8 %all-gather.20.cloned.1.call-start = ((), (), s32[]{:S(2)}) async-start(), calls=%async_computation.9 | async-start | bytes 9437184 | tf_op jit(solution)/shard_map/all_gather | solution.py:197
  303.8 319.1 %copy-start.2 = (bf16[128,2048]{1,0:T(8,128)(2,1)S(1)}, bf16[128,2048]{1,0:T(8,128)(2,1)}, u32[]{:S(2)}) copy-start(bf16[128,2048]{1,0:T(8,128)(2,1)} %reduce-scatter.3.cloned.1.call-done) | copy-start | bytes 1572868
  303.8 319.1 %reduce-scatter.5.cloned.1.call-start = ((), (), s32[]{:S(2)}) async-start(), calls=%async_computation.10 | async-start | bytes 2621440 | tf_op jit(solution)/shard_map/reduce_scatter | solution.py:198
Sparse Core Ops, SparseCore 0:
  9.4 45.6 all-gather.11
  57.1 40.3 all-gather.13
  99.5 49.2 all-gather.9
  150.7 48.5 all-gather.7
  268.5 30.3 reduce-scatter.2
  302.4 22.5 all-gather.15
  327.1 124.4 all-gather.17
  453.7 123.1 all-gather.19
  593.5 29.3 reduce-scatter.4
where the time goes:
time: 633 us; the launch traced here: 631 us
  waiting for transfers between devices  485 us (77%)
  matrix products  47.3 us (7%)
  local copies, waits for them, and re-layouts  43.4 us (7%)
  other arithmetic  19.2 us (3%)
  between operations  18.8 us (3%)
  starting transfers between devices  11 us (2%)
  loops' own time  6.78 us (1%)
    all_gather x1, waiting for transfers between devices, body(): lax.all_gather(up_weight, 'sp', axis=0, tiled=True)  127 us
    all_gather x1, waiting for transfers between devices, body(): down_full = lax.all_gather(down_weight, 'sp', axis=1, tiled=True)  125 us
    all_gather x1, waiting for transfers between devices, body(): lax.all_gather(keys_major, 'sp', axis=0, tiled=True)  50.5 us
    all_gather x1, waiting for transfers between devices, body(): lax.all_gather(values_minor, 'sp', axis=0, tiled=True)  42.4 us
    ppermute x6, waiting for transfers between devices, swapped(): return lax.ppermute(value, axis, pairs)  34 us
    dynamic_slice x34, local copies, waits for them, and re-layouts, update(): values_block = lax.dynamic_slice_in_dim(values, key_first, block_len, 0)  32 us
    reduce_scatter x1, waiting for transfers between devices, body(): lax.psum_scatter(to_wire(partial_sum).astype(jnp.bfloat16), 'tp', scatter...  30.5 us
    reduce_scatter x1, waiting for transfers between devices, body(): lax.psum_scatter(to_wire(jnp.dot(hidden, down_full, preferred_element_typ...  29.5 us
  transfers between devices with their start and end apart: 15, of which 15 were waited for; matrix products, arithmetic and copies ran while one was open for 7% of the time, Pallas kernels for 0%

commit v1 on v0

--- a/solution.py
+++ b/solution.py
@@ -8,6 +8,13 @@
 SEGMENT = 64
 EPSILON = 1e-06
 NEGATIVE = -1e30
+
+
+def swapped_in(value, axis, along):
+    n_dev = lax.axis_size(axis)
+    pieces = jnp.stack([value for _ in range(n_dev)])
+    pieces = lax.all_to_all(pieces, axis, split_axis=0, concat_axis=0)
+    return jnp.concatenate(pieces, axis=along)
 
 
 def swapped(value, axis, stride):
@@ -151,7 +158,7 @@
     )
     fold_pieces = (
         lax.all_gather(keys_minor, "sp", axis=0, tiled=True),
-        lax.all_gather(values_minor, "sp", axis=0, tiled=True),
+        swapped_in(values_minor, "sp", 0),
     )
     first_major = finish(
         fold_piece(init_major[0], early_major, pieces[0], pieces[1], early_pos, DK_MAJOR),

time: 633 us -> 604 us (0.954)
  waiting for transfers between devices: 485 us -> 449 us
  starting transfers between devices: 11 us -> 19.8 us
    all_gather x1 -> x0, waiting for transfers between devices: 42.4 us -> none  [body(): lax.all_gather(values_minor, 'sp', axis=0, tiled=True)]
    all_gather x1, waiting for transfers between devices: 14.2 us -> 50.6 us  [body(): lax.all_gather(values_major, 'sp', axis=0, tiled=True)]
    all_gather x1, waiting for transfers between devices: 50.5 us -> 15.3 us  [body(): lax.all_gather(keys_major, 'sp', axis=0, tiled=True)]
    ppermute x6, waiting for transfers between devices: 34 us -> 46.8 us  [swapped(): return lax.ppermute(value, axis, pairs)]
    all_gather x1, waiting for transfers between devices: 9.58 us -> 1.74 us  [body(): lax.all_gather(keys_minor, 'sp', axis=0, tiled=True)]
    all_to_all x0 -> x1, starting transfers between devices: none -> 7.31 us  [swapped_in(): pieces = lax.all_to_all(pieces, axis, split_axis=0, concat_axis=0)]
  transfers between devices with their start and end apart: 15 -> 15, of which waited for: 15 -> 14; matrix products, arithmetic and copies ran while one was open for 7% -> 7% of each run, Pallas kernels for 0% -> 0%
where the time goes in v1:
time: 604 us; the launch traced here: 602 us
  waiting for transfers between devices  449 us (74%)
  matrix products  47.3 us (8%)
  local copies, waits for them, and re-layouts  43.1 us (7%)
  starting transfers between devices  19.8 us (3%)
  between operations  18.8 us (3%)
  other arithmetic  17.9 us (3%)
  loops' own time  6.78 us (1%)
    all_gather x1, waiting for transfers between devices, body(): lax.all_gather(up_weight, 'sp', axis=0, tiled=True)  126 us
    all_gather x1, waiting for transfers between devices, body(): down_full = lax.all_gather(down_weight, 'sp', axis=1, tiled=True)  125 us
    all_gather x1, waiting for transfers between devices, body(): lax.all_gather(values_major, 'sp', axis=0, tiled=True)  50.6 us
    ppermute x6, waiting for transfers between devices, swapped(): return lax.ppermute(value, axis, pairs)  46.8 us
    dynamic_slice x34, local copies, waits for them, and re-layouts, update(): values_block = lax.dynamic_slice_in_dim(values, key_first, block_len, 0)  32 us
    reduce_scatter x1, waiting for transfers between devices, body(): lax.psum_scatter(to_wire(partial_sum).astype(jnp.bfloat16), 'tp', scatter...  30.4 us
    reduce_scatter x1, waiting for transfers between devices, body(): lax.psum_scatter(to_wire(jnp.dot(hidden, down_full, preferred_element_typ...  29.5 us
    all_gather x1, waiting for transfers between devices, body(): lax.all_gather(normalize(stream, mixer_gain), 'tp', axis=0, tiled=True)  21.2 us
  transfers between devices with their start and end apart: 15, of which 14 were waited for; matrix products, arithmetic and copies ran while one was open for 7% of the time, Pallas kernels for 0%

profile of v1, /device:TPU:0, one launch (start us, length us, event | category | flops | bytes accessed | tf_op | source)
XLA Modules:
  0.0 602.1 jit_solution(16024482495308305158)
XLA Ops:
  12.3 7.3 %all-to-all-start = ((bf16[8,512,128]{1,2,0:T(8,128)(2,1)}), bf16[8,512,128]{1,2,0:T(8,128)(2,1)S(1)}, u32[]{:S(2)}, u32[]{:S(2)}) async-start(bf16[8,512,128]{1,2,0:T(8,128)(2,1)} %stack.2), calls=%async_computation | async-start | bytes 2097152 | tf_op jit(solution)/shard_map/all_to_all | solution.py:16
  20.7 2.0 collective-permute-start
  22.8 12.8 %collective-permute-done = bf16[256,384]{1,0:T(8,128)(2,1)S(1)} collective-permute-done((bf16[256,384]{1,0:T(8,128)(2,1)S(1)}, bf16[256,384]{1,0:T(8,128)(2,1)S(1)}, u32[]{:S(2)}, u32[]{:S(2)}) %collective-permute-start) | collective-permute-done | bytes 196640 | tf_op jit(solution)/shard_map/ppermute | solution.py:23
  35.6 9.5 %collective-permute-done.1 = bf16[256,384]{1,0:T(8,128)(2,1)S(1)} collective-permute-done((bf16[256,384]{1,0:T(8,128)(2,1)S(1)}, bf16[256,384]{1,0:T(8,128)(2,1)S(1)}, u32[]{:S(2)}, u32[]{:S(2)}) %collective-permute-start.1) | collective-permute-done | bytes 196640 | tf_op jit(solution)/shard_map/ppermute | solution.py:23
  45.1 7.4 %collective-permute-start.2 = (bf16[256,384]{1,0:T(8,128)(2,1)S(1)}, bf16[256,384]{1,0:T(8,128)(2,1)S(1)}, u32[]{:S(2)}, u32[]{:S(2)}) collective-permute-start(bf16[256,384]{1,0:T(8,128)(2,1)S(1)} %collective-permute-done.1), channel_id=1, source_target_pairs={{0,16},{4,20},{8,24},{12,28},{16,0},{20,4},{24,8},{28,12},{1,17},{... | collective-permute-start | bytes 589832 | tf_op jit(solution)/shard_map/ppermute | solution.py:23
  58.8 5.2 collective-permute-done.2
  68.0 33.4 %while.82 = (s32[]{:T(128)}, f32[2,2,256]{2,1,0:T(2,128)S(1)}, f32[2,2,256]{2,1,0:T(2,128)S(1)}, f32[2,2,256,64]{2,3,1,0:T(8,128)S(1)}, s32[]{:T(128)}, /*index=...) while((s32[]{:T(128)}, f32[2,2,256]{2,1,0:T(2,128)S(1)}, ...), condition=%wide.region_19.20_spmd.clone, body=%wide.region_14.19_spmd.clone.sunk | while | flops 52897816 | bytes 4463083 | solution.py:79
  68.1 2.0 conditional.14
  70.2 2.0 conditional.14
  74.3 2.0 conditional.14
  76.4 2.0 conditional.14
  89.0 2.0 conditional.14
  91.0 2.0 conditional.14
  97.3 2.0 conditional.14
  101.5 3.3 while.83
  105.1 15.3 %all-gather.7.cloned.1.call-done = bf16[4096,256]{0,1:T(8,128)(2,1)} async-done(((bf16[512,256]{0,1:T(8,128)(2,1)}), bf16[4096,256]{0,1:T(8,128)(2,1)}) %all-gather.7.cloned.1.call-update) | async-done | bytes 2097168 | tf_op jit(solution)/shard_map/all_gather | solution.py:156
  120.5 50.6 %all-gather.9.cloned.1.call-done = bf16[4096,256]{0,1:T(8,128)(2,1)} async-done(((bf16[512,256]{0,1:T(8,128)(2,1)}), bf16[4096,256]{0,1:T(8,128)(2,1)}) %all-gather.9.cloned.1.call-update) | async-done | bytes 2097168 | tf_op jit(solution)/shard_map/all_gather | solution.py:157
  171.1 38.5 %while.81 = (s32[]{:T(128)}, f32[2,2,256]{2,1,0:T(2,128)S(1)}, f32[2,2,256]{2,1,0:T(2,128)S(1)}, f32[2,2,256,128]{3,2,1,0:T(8,128)S(1)}, s32[]{:T(128)}, /*index...) while((s32[]{:T(128)}, f32[2,2,256]{2,1,0:T(2,128)S(1)}, ...), condition=%wide.region_12.13_spmd.clone, body=%wide.region_7.12_spmd.clone.sunk | while | flops 103360528 | bytes 5446123 | solution.py:79
  171.2 2.3 conditional.13
  173.6 2.3 conditional.13
  176.0 2.3 conditional.13
  178.4 2.3 conditional.13
  180.8 2.3 conditional.13
  183.2 2.3 conditional.13
  185.6 2.3 conditional.13
  188.1 2.3 conditional.13
  190.5 2.3 conditional.13
  192.9 2.3 conditional.13
  195.3 2.3 conditional.13
  197.7 2.3 conditional.13
  200.1 2.3 conditional.13
  202.5 2.3 conditional.13
  204.9 2.3 conditional.13
  207.3 2.3 conditional.13
  209.8 3.6 while.80
  209.8 2.3 conditional.12
  215.7 5.0 collective-permute-done.3
  220.7 5.7 collective-permute-done.4
  227.4 8.6 %collective-permute-done.5 = bf16[256,384]{0,1:T(8,128)(2,1)S(1)} collective-permute-done((bf16[256,384]{0,1:T(8,128)(2,1)S(1)}, bf16[256,384]{0,1:T(8,128)(2,1)S(1)}, u32[]{:S(2)}, u32[]{:S(2)}) %collective-permute-start.5) | collective-permute-done | bytes 196640 | tf_op jit(solution)/shard_map/ppermute | solution.py:23
  236.8 2.1 add_convert_fusion
  238.9 30.4 %reduce-scatter.3.cloned.1.call-done = bf16[128,2048]{1,0:T(8,128)(2,1)} async-done(((bf16[512,2048]{1,0:T(8,128)(2,1)}), bf16[128,2048]{1,0:T(8,128)(2,1)}) %reduce-scatter.3.cloned.1.call-update) | async-done | bytes 524304 | tf_op jit(solution)/shard_map/reduce_scatter | solution.py:193
  270.7 2.0 multiply_convert_fusion.1
  274.3 21.2 %all-gather.13.cloned.1.call-done = bf16[512,2048]{1,0:T(8,128)(2,1)} async-done(((bf16[128,2048]{1,0:T(8,128)(2,1)}), bf16[512,2048]{1,0:T(8,128)(2,1)}) %all-gather.13.cloned.1.call-update) | async-done | bytes 2097168 | tf_op jit(solution)/shard_map/all_gather | solution.py:197
  295.5 126.5 %all-gather.15.cloned.1.call-done = bf16[2048,2048]{1,0:T(8,128)(2,1)} async-done(((bf16[256,2048]{1,0:T(8,128)(2,1)}), bf16[2048,2048]{1,0:T(8,128)(2,1)}) %all-gather.15.cloned.1.call-update) | async-done | bytes 8388624 | tf_op jit(solution)/shard_map/all_gather | solution.py:200
  422.0 125.2 %all-gather.17.cloned.1.call-done = bf16[2048,2048]{1,0:T(8,128)(2,1)} async-done(((bf16[2048,256]{1,0:T(8,128)(2,1)}), bf16[2048,2048]{1,0:T(8,128)(2,1)}) %all-gather.17.cloned.1.call-update) | async-done | bytes 8388624 | tf_op jit(solution)/shard_map/all_gather | solution.py:204
  547.2 16.5 %convolution_convert_fusion = bf16[512,2048]{1,0:T(8,128)(2,1)} fusion(bf16[2048,2048]{1,0:T(8,128)(2,1)} %all-gather.17.cloned.1.call-done, bf16[512,2048]{1,0:T(8,128)(2,1)} %all-gather.13.cloned.1.call-done, bf16[2048,2048]{1,0:T(8,128)(2,1)} %all-gather.15.cloned.1.call-done), kind=kOutput, calls=%fused_computation.102 | convolution fusion | flops 8594128896 | bytes 20971520 | tf_op jit(solution)/shard_map/dot_general | solution.py:206
  563.7 29.5 %reduce-scatter.5.cloned.1.call-done = bf16[128,2048]{1,0:T(8,128)(2,1)} async-done(((bf16[512,2048]{1,0:T(8,128)(2,1)}), bf16[128,2048]{1,0:T(8,128)(2,1)}) %reduce-scatter.5.cloned.1.call-update) | async-done | bytes 524304 | tf_op jit(solution)/shard_map/reduce_scatter | solution.py:205
  593.2 2.1 add_convert_fusion.1
  (512 shorter events, 112.4 us)
Async XLA Ops:
  6.5 230.2 %copy-start = (bf16[256,2048]{1,0:T(8,128)(2,1)S(1)}, bf16[256,2048]{1,0:T(8,128)(2,1)}, u32[]{:S(2)}) copy-start(bf16[256,2048]{1,0:T(8,128)(2,1)} %param.43) | copy-start | bytes 3145732
  6.5 13.2 %copy-start.4 = (bf16[512,256]{1,0:T(8,128)(2,1)S(1)}, bf16[512,256]{1,0:T(8,128)(2,1)}, u32[]{:S(2)}) copy-start(bf16[512,256]{1,0:T(8,128)(2,1)} %param.35) | copy-start | bytes 786436
  6.5 14.1 %copy-start.6 = (bf16[512,128]{1,0:T(8,128)(2,1)S(1)}, bf16[512,128]{1,0:T(8,128)(2,1)}, u32[]{:S(2)}) copy-start(bf16[512,128]{1,0:T(8,128)(2,1)} %param.36) | copy-start | bytes 393220
  6.5 14.1 %copy-start.5 = (bf16[512,256]{1,0:T(8,128)(2,1)S(1)}, bf16[512,256]{1,0:T(8,128)(2,1)}, u32[]{:S(2)}) copy-start(bf16[512,256]{1,0:T(8,128)(2,1)} %param.33) | copy-start | bytes 786436
  6.5 61.4 %all-gather.11.cloned.1.call-start = ((), (), s32[]{:S(2)}) async-start(), calls=%async_computation.5 | async-start | bytes 1179648 | tf_op jit(solution)/shard_map/all_gather | solution.py:160
  8.4 112.1 %all-gather.7.cloned.1.call-start = ((), (), s32[]{:S(2)}) async-start(), calls=%async_computation.3 | async-start | bytes 2359296 | tf_op jit(solution)/shard_map/all_gather | solution.py:156
  12.3 51.9 %all-to-all-start = ((bf16[8,512,128]{1,2,0:T(8,128)(2,1)}), bf16[8,512,128]{1,2,0:T(8,128)(2,1)S(1)}, u32[]{:S(2)}, u32[]{:S(2)}) async-start(bf16[8,512,128]{1,2,0:T(8,128)(2,1)} %stack.2), calls=%async_computation | async-start | bytes 2097152 | tf_op jit(solution)/shard_map/all_to_all | solution.py:16
  19.7 151.4 %all-gather.9.cloned.1.call-start = ((), (), s32[]{:S(2)}) async-start(), calls=%async_computation.4 | async-start | bytes 2359296 | tf_op jit(solution)/shard_map/all_gather | solution.py:157
  20.6 248.8 %reduce-scatter.3.cloned.1.call-start = ((), (), s32[]{:S(2)}) async-start(), calls=%async_computation.6 | async-start | bytes 2621440 | tf_op jit(solution)/shard_map/reduce_scatter | solution.py:193
  20.7 14.8 %collective-permute-start = (bf16[256,384]{1,0:T(8,128)(2,1)S(1)}, bf16[256,384]{1,0:T(8,128)(2,1)S(1)}, u32[]{:S(2)}, u32[]{:S(2)}) collective-permute-start(bf16[256,384]{1,0:T(8,128)(2,1)S(1)} %pad_maximum_fusion), channel_id=1, source_target_pairs={{0,4},{4,0},{8,12},{12,8},{16,20},{20,16},{24,28},{28,24},{1,5},{5... | collective-permute-start | bytes 589832 | tf_op jit(solution)/shard_map/ppermute | solution.py:23
  35.5 9.6 %collective-permute-start.1 = (bf16[256,384]{1,0:T(8,128)(2,1)S(1)}, bf16[256,384]{1,0:T(8,128)(2,1)S(1)}, u32[]{:S(2)}, u32[]{:S(2)}) collective-permute-start(bf16[256,384]{1,0:T(8,128)(2,1)S(1)} %collective-permute-done), channel_id=1, source_target_pairs={{0,8},{4,12},{8,0},{12,4},{16,24},{20,28},{24,16},{28,20},{1,9},{5... | collective-permute-start | bytes 589832 | tf_op jit(solution)/shard_map/ppermute | solution.py:23
  45.1 18.8 %collective-permute-start.2 = (bf16[256,384]{1,0:T(8,128)(2,1)S(1)}, bf16[256,384]{1,0:T(8,128)(2,1)S(1)}, u32[]{:S(2)}, u32[]{:S(2)}) collective-permute-start(bf16[256,384]{1,0:T(8,128)(2,1)S(1)} %collective-permute-done.1), channel_id=1, source_target_pairs={{0,16},{4,20},{8,24},{12,28},{16,0},{20,4},{24,8},{28,12},{1,17},{... | collective-permute-start | bytes 589832 | tf_op jit(solution)/shard_map/ppermute | solution.py:23
  101.5 3.4 copy-start.10
  101.5 3.5 copy-start.8
  209.8 4.1 copy-start.9
  209.8 4.3 copy-start.11
  213.4 22.6 %copy-start.3 = (bf16[128,2048]{1,0:T(8,128)(2,1)S(1)}, bf16[128,2048]{1,0:T(8,128)(2,1)}, u32[]{:S(2)}) copy-start(bf16[128,2048]{1,0:T(8,128)(2,1)} %param.44) | copy-start | bytes 1572868
  214.2 6.5 %collective-permute-start.3 = (bf16[256,384]{0,1:T(8,128)(2,1)S(1)}, bf16[256,384]{0,1:T(8,128)(2,1)S(1)}, u32[]{:S(2)}, u32[]{:S(2)}) collective-permute-start(bf16[256,384]{0,1:T(8,128)(2,1)S(1)} %pad_maximum_fusion.1), channel_id=1, source_target_pairs={{0,4},{4,0},{8,12},{12,8},{16,20},{20,16},{24,28},{28,24},{1,5},{5... | collective-permute-start | bytes 589832 | tf_op jit(solution)/shard_map/ppermute | solution.py:23
  220.7 5.7 collective-permute-start.4
  226.4 9.6 %collective-permute-start.5 = (bf16[256,384]{0,1:T(8,128)(2,1)S(1)}, bf16[256,384]{0,1:T(8,128)(2,1)S(1)}, u32[]{:S(2)}, u32[]{:S(2)}) collective-permute-start(bf16[256,384]{0,1:T(8,128)(2,1)S(1)} %collective-permute-done.4), channel_id=1, source_target_pairs={{0,16},{4,20},{8,24},{12,28},{16,0},{20,4},{24,8},{28,12},{1,17},{... | collective-permute-start | bytes 589832 | tf_op jit(solution)/shard_map/ppermute | solution.py:23
  236.7 32.7 %copy-start.1 = (bf16[128,2048]{1,0:T(8,128)(2,1)S(1)}, bf16[128,2048]{1,0:T(8,128)(2,1)}, u32[]{:S(2)}) copy-start(bf16[128,2048]{1,0:T(8,128)(2,1)} %param.32) | copy-start | bytes 1572868
  236.8 34.0 %copy-start.7 = (f32[2048]{0:T(1024)S(1)}, f32[2048]{0:T(1024)}, u32[]{:S(2)}) copy-start(f32[2048]{0:T(1024)} %param.45) | copy-start | bytes 24580
  238.9 56.6 %all-gather.13.cloned.1.call-start = ((), (), s32[]{:S(2)}) async-start(), calls=%async_computation.7 | async-start | bytes 2621440 | tf_op jit(solution)/shard_map/all_gather | solution.py:197
  272.8 149.2 %all-gather.15.cloned.1.call-start = ((), (), s32[]{:S(2)}) async-start(), calls=%async_computation.8 | async-start | bytes 9437184 | tf_op jit(solution)/shard_map/all_gather | solution.py:200
  273.4 273.8 %all-gather.17.cloned.1.call-start = ((), (), s32[]{:S(2)}) async-start(), calls=%async_computation.9 | async-start | bytes 9437184 | tf_op jit(solution)/shard_map/all_gather | solution.py:204
  274.1 319.1 %copy-start.2 = (bf16[128,2048]{1,0:T(8,128)(2,1)S(1)}, bf16[128,2048]{1,0:T(8,128)(2,1)}, u32[]{:S(2)}) copy-start(bf16[128,2048]{1,0:T(8,128)(2,1)} %reduce-scatter.3.cloned.1.call-done) | copy-start | bytes 1572868
  274.1 319.1 %reduce-scatter.5.cloned.1.call-start = ((), (), s32[]{:S(2)}) async-start(), calls=%async_computation.10 | async-start | bytes 2621440 | tf_op jit(solution)/shard_map/reduce_scatter | solution.py:205
Sparse Core Ops, SparseCore 0:
  9.4 58.5 all-gather.10
  70.0 50.4 all-gather.6
  122.5 48.5 all-gather.8
  239.0 30.3 reduce-scatter.2
  272.9 22.5 all-gather.12
  297.5 124.4 all-gather.14
  424.0 123.1 all-gather.16
  563.8 29.3 reduce-scatter.4
